TPU v7x, 32 devices: a whole 2x2x4 slice. The times are simulated.
32 devices in a mesh: rep: 2 (over y), fs: 4 (over z), tp: 4 (over x, core).
Axes of the slice: x: 2, y: 2, z: 4, core: 2. Of those that a mesh axis runs over, the one named last changes fastest.
Arguments:
- tokens: bfloat16 [8, 512, 2048], P(('rep', 'fs')), may hold values from -6 to 6
- first_gain: float32 [2048], replicated, may hold values from 0.1 to 1.9
- in_matrix: float32 [2048, 2048], P('fs', 'tp'), may hold values from -0.125 to 0.125
- in_scale: float32 [2048], P('tp'), may hold values from 0.5 to 2
- conv_taps: float32 [4, 2048], P(None, 'tp'), may hold values from -3 to 3
- decay_rate: float32 [2, 2048], P(None, 'tp'), may hold values from 0 to 1, as said below
- recall_maps: float32 [2, 8, 256, 256], P(None, 'tp'), may hold values from -0.375 to 0.375
- admit_maps: float32 [2, 8, 256, 256], P(None, 'tp'), may hold values from -0.375 to 0.375
- out_matrix: float32 [2048, 2048], P('fs', 'tp'), may hold values from -0.125 to 0.125
- out_scale: float32 [2048], P('fs'), may hold values from 0.5 to 2
- second_gain: float32 [2048], replicated, may hold values from 0.1 to 1.9
- up_matrix: float32 [2048, 4096], P('fs', 'tp'), may hold values from -0.125 to 0.125
- up_scale: float32 [4096], P('tp'), may hold values from 0.5 to 2
- down_matrix: float32 [2048, 4096], P('fs', 'tp'), may hold values from -0.09375 to 0.09375
- down_scale: float32 [2048], P('fs'), may hold values from 0.5 to 2
Outputs:
- layer_out: bfloat16 [8, 512, 2048], P(('rep', 'fs'))
Inputs may be any that keep to these rules, and one draw needn't show every extreme that they name: `decay_rate`: positive per-step decay rates.
All inputs are finite; a program needn't handle non-finite values.
Results may differ from a plain program's by a relative error of at most 0.024.
Values may be sent and summed in bfloat16 or wider, within the bound.
A program may use at most 64 MiB of HBM per device.

v0:
```python
import jax
import jax.numpy as jnp
from jax import lax
from jax.sharding import PartitionSpec as P

EPSILON = 1e-06
RATE_GAIN = 8.0


def normalize(stream, gain):
    return stream * lax.rsqrt(jnp.mean(stream * stream, axis=-1, keepdims=True) + EPSILON) * gain


def convolve(values, taps):
    length = values.shape[0]
    count = taps.shape[0]
    padded = jnp.pad(values, ((count // 2, count - 1 - count // 2), (0, 0)))
    total = taps[0] * padded[0:length]
    for offset in range(1, count):
        total = total + taps[offset] * padded[offset : offset + length]
    return total


def block_map(values, maps):
    length = values.shape[0]
    count, width = (maps.shape[0], maps.shape[1])
    grouped = values.reshape(length, count, width)
    mapped = jnp.einsum("lnj,njk->lnk", grouped, maps, precision=lax.Precision.HIGHEST)
    return mapped.reshape(length, count * width)


def combine_steps(earlier, later):
    return (earlier[0] * later[0], later[0] * earlier[1] + later[1])


def one_direction(values, rate, recall_map, admit_map):
    recall = jax.nn.sigmoid(block_map(values, recall_map))
    admit = jax.nn.sigmoid(block_map(values, admit_map))
    log_decay = -RATE_GAIN * recall * rate
    decay = jnp.exp(log_decay)
    drive = jnp.sqrt(-jnp.expm1(2.0 * log_decay)) * admit * values
    carried = lax.associative_scan(combine_steps, (decay, drive), axis=0)
    return carried[1]


def recurrence(values, rates, recall_maps, admit_maps):
    forward = one_direction(values, rates[0], recall_maps[0], admit_maps[0])
    backward = one_direction(values[::-1], rates[1], recall_maps[1], admit_maps[1])[::-1]
    return forward + backward


def contract_last(left, right):
    return lax.dot_general(
        left, right, (((1,), (1,)), ((), ())), preferred_element_type=jnp.float32
    )


def body(
    tokens,
    first_gain,
    in_matrix,
    in_scale,
    conv_taps,
    decay_rate,
    recall_maps,
    admit_maps,
    out_matrix,
    out_scale,
    second_gain,
    up_matrix,
    up_scale,
    down_matrix,
    down_scale,
):
    stream = tokens.reshape(tokens.shape[1], tokens.shape[2]).astype(jnp.float32)
    in_cols, out_rows, out_factor, down_factor = (
        lax.all_gather(in_matrix.astype(jnp.bfloat16), "fs", axis=0, tiled=True),
        lax.all_gather(out_matrix.astype(jnp.bfloat16), "fs", axis=0, tiled=True),
        lax.all_gather(out_scale.astype(jnp.bfloat16), "fs", axis=0, tiled=True),
        lax.all_gather(down_scale.astype(jnp.bfloat16), "fs", axis=0, tiled=True),
    )
    normed = normalize(stream, first_gain).astype(jnp.bfloat16)
    before = (
        jnp.dot(normed, in_cols, preferred_element_type=jnp.float32) * in_scale.astype(jnp.bfloat16)
    ).astype(jnp.bfloat16)
    conv_out = convolve(before.astype(jnp.float32), conv_taps)
    mixed = recurrence(conv_out, decay_rate, recall_maps, admit_maps).astype(jnp.bfloat16)
    partial_value = contract_last(mixed, out_rows)
    middle = stream + out_factor * lax.psum(partial_value.astype(jnp.bfloat16), "tp").astype(
        jnp.float32
    )
    second_normed = normalize(middle, second_gain).astype(jnp.bfloat16)
    raised = jnp.dot(
        second_normed,
        lax.all_gather(up_matrix.astype(jnp.bfloat16), "fs", axis=0, tiled=True),
        preferred_element_type=jnp.float32,
    )
    active = jnp.square(jax.nn.relu(raised * up_scale.astype(jnp.bfloat16))).astype(jnp.bfloat16)
    lowered = contract_last(
        active, lax.all_gather(down_matrix.astype(jnp.bfloat16), "fs", axis=0, tiled=True)
    )
    result = (
        middle + down_factor * lax.psum(lowered.astype(jnp.bfloat16), "tp").astype(jnp.float32)
    ).astype(jnp.bfloat16)
    return result.reshape(tokens.shape)


def solution(mesh):
    placed = (
        P(("rep", "fs"), None, None),
        P(),
        P("fs", "tp"),
        P("tp"),
        P(None, "tp"),
        P(None, "tp"),
        P(None, "tp", None, None),
        P(None, "tp", None, None),
        P("fs", "tp"),
        P("fs"),
        P(),
        P("fs", "tp"),
        P("tp"),
        P("fs", "tp"),
        P("fs"),
    )
    return jax.shard_map(
        body, mesh=mesh, in_specs=placed, out_specs=P(("rep", "fs"), None, None), check_vma=False
    )
```

profile of v0, /device:TPU:0, one launch (start us, length us, event | category | flops | bytes accessed | tf_op | source)
XLA Modules:
  0.0 626.4 jit_solution(6509741155508411147)
XLA Ops:
  6.5 2.2 convert_element_type.82
  11.0 46.4 %all-gather.7.cloned.1.call-done = bf16[2048,512]{1,0:T(8,128)(2,1)} async-done(((bf16[512,512]{1,0:T(8,128)(2,1)}), bf16[2048,512]{1,0:T(8,128)(2,1)}) %all-gather.7.cloned.1.call-update) | async-done | bytes 2097168 | tf_op jit(solution)/shard_map/all_gather | solution.py:77
  57.3 2.9 fusion.32
  62.2 2.3 fusion.28
  64.6 2.6 copy.40
  67.2 3.3 fusion.25
  70.5 2.6 copy.41
  73.0 5.3 multiply_exponential_fusion.1
  78.3 2.1 slice.467
  80.4 2.1 slice.468
  82.5 3.7 slice.466
  86.1 3.7 slice.470
  89.8 2.7 fusion.73
  92.5 2.5 slice.473
  95.0 2.5 slice.474
  97.5 2.5 slice.472
  100.0 2.5 slice.476
  102.5 2.0 fusion.75
  107.5 1.6 slice.482
  109.1 1.8 fusion.77
  158.1 1.6 slice.477
  161.0 2.5 slice.528
  163.6 2.5 slice.471
  167.4 2.1 slice.530
  169.5 3.7 slice.465
  173.8 6.8 %rev.6 = f32[512,512]{1,0:T(8,128)S(1)} reverse(f32[512,512]{1,0:T(8,128)} %copy-done.4), dimensions={0} | reverse | bytes 2097152 | tf_op jit(solution)/shard_map/rev | solution.py:48
  180.6 3.7 fusion.22
  184.3 2.3 fusion.19
  186.6 2.6 copy.42
  190.5 3.6 multiply_exponential_fusion
  194.1 2.1 slice.537
  196.2 2.1 slice.538
  198.2 3.6 slice.536
  201.9 3.6 slice.540
  205.5 2.7 fusion.74
  208.2 2.5 slice.543
  210.7 2.5 slice.544
  213.2 2.5 slice.542
  215.7 2.5 slice.546
  218.2 2.0 fusion.76
  224.8 1.8 fusion.78
  270.5 1.6 slice.547
  273.5 1.9 slice.598
  275.4 2.5 slice.541
  279.3 2.1 slice.600
  281.4 3.7 slice.535
  298.7 4.6 pad.132
  304.9 2.7 pad.131
  315.7 4.6 pad.150
  321.8 2.7 pad.149
  324.5 2.8 add.359
  327.3 9.0 %rev.7 = f32[512,512]{1,0:T(8,128)} reverse(f32[512,512]{1,0:T(8,128)} %add.359), dimensions={0} | reverse | bytes 2097152 | tf_op jit(solution)/shard_map/rev | solution.py:48
  336.3 4.9 convolution_convert_fusion.1
  341.2 2.8 convert_element_type.94
  344.1 2.9 convert_element_type.98
  347.1 11.9 %all-gather = bf16[4,1,512]{2,1,0:T(2,128)(2,1)S(1)} all-gather(bf16[1,1,512]{2,1,0:T(2,128)(2,1)S(1)} %reshape.72), channel_id=1, replica_groups=mesh['rep'=2,'fs'=4,'tp'=4] {'fs'}, dimensions={0}, use_global_device_ids=true | all-gather | bytes 5120 | tf_op jit(solution)/shard_map/all_gather | solution.py:79
  359.1 32.4 %all-reduce.40.cloned.1.call-done = bf16[512,2048]{1,0:T(8,128)(2,1)} async-done(((bf16[512,2048]{1,0:T(8,128)(2,1)}), bf16[512,2048]{1,0:T(8,128)(2,1)}) %all-reduce.40.cloned.1.call-update) | async-done | bytes 2097168 | tf_op jit(solution)/shard_map/psum | solution.py:89
  391.5 2.5 multiply_reduce_fusion
  394.0 79.8 %all-gather.11.cloned.1.call-done = bf16[2048,1024]{1,0:T(8,128)(2,1)} async-done(((bf16[512,1024]{1,0:T(8,128)(2,1)}), bf16[2048,1024]{1,0:T(8,128)(2,1)}) %all-gather.11.cloned.1.call-update) | async-done | bytes 4194320 | tf_op jit(solution)/shard_map/all_gather | solution.py:95
  473.8 80.7 %all-gather.13.cloned.1.call-done = bf16[2048,1024]{1,0:T(8,128)(2,1)} async-done(((bf16[512,1024]{1,0:T(8,128)(2,1)}), bf16[2048,1024]{1,0:T(8,128)(2,1)}) %all-gather.13.cloned.1.call-update) | async-done | bytes 4194320 | tf_op jit(solution)/shard_map/all_gather | solution.py:100
  554.4 9.9 %convolution_convert_fusion = bf16[512,2048]{1,0:T(8,128)(2,1)} fusion(bf16[2048,1024]{1,0:T(8,128)(2,1)} %all-gather.13.cloned.1.call-done, bf16[2048,1024]{1,0:T(8,128)(2,1)} %all-gather.11.cloned.1.call-done, bf16[512,2048]{1,0:T(8,128)(2,1)} %all-reduce.40.cloned.1.call-done, bf16[1,512,2048]{2,1,0:T(8,128)(2,1)S(1)} %copy-done, ...), kind=kOutput, calls=%fused_computation.9 | convolution fusion | flops 4305453056 | bytes 14702592 | tf_op jit(solution)/shard_map/dot_general | solution.py:53
  565.1 11.9 %all-gather.1 = bf16[4,1,512]{2,1,0:T(2,128)(2,1)S(1)} all-gather(bf16[1,1,512]{2,1,0:T(2,128)(2,1)S(1)} %reshape.74), channel_id=1, replica_groups=mesh['rep'=2,'fs'=4,'tp'=4] {'fs'}, dimensions={0}, use_global_device_ids=true | all-gather | bytes 5120 | tf_op jit(solution)/shard_map/all_gather | solution.py:80
  577.0 37.4 %all-reduce.42.cloned.1.call-done = bf16[512,2048]{1,0:T(8,128)(2,1)} async-done(((bf16[512,2048]{1,0:T(8,128)(2,1)}), bf16[512,2048]{1,0:T(8,128)(2,1)}) %all-reduce.42.cloned.1.call-update) | async-done | bytes 2097168 | tf_op jit(solution)/shard_map/psum | solution.py:103
  614.4 5.1 fusion.4
  (277 shorter events, 135.1 us)
Async XLA Ops:
  6.5 2.4 copy-start.8
  6.5 3.3 copy-start.31
  6.5 3.3 copy-start
  6.5 50.8 %all-gather.7.cloned.1.call-start = ((), (), s32[]{:S(2)}) async-start(), calls=%async_computation | async-start | bytes 2621440 | tf_op jit(solution)/shard_map/all_gather | solution.py:77
  8.8 1.5 copy-start.32
  8.8 2.1 copy-start.36
  8.8 48.5 %copy-start.39 = (f32[2048]{0:T(1024)S(1)}, f32[2048]{0:T(1024)}, u32[]{:S(2)}) copy-start(f32[2048]{0:T(1024)} %param.16) | copy-start | bytes 24580
  8.8 327.4 %all-gather.9.cloned.1.call-start = ((), (), s32[]{:S(2)}) async-start(), calls=%async_computation.1 | async-start | bytes 2621440 | tf_op jit(solution)/shard_map/all_gather | solution.py:78
  9.8 381.7 %all-reduce.40.cloned.1.call-start = ((), (), s32[]{:S(2)}) async-start(), calls=%async_computation.2 | async-start | bytes 4194304 | tf_op jit(solution)/shard_map/psum | solution.py:89
  60.2 4.3 copy-start.2
  60.2 2.0 copy-start.37
  60.7 6.5 %copy-start.4 = (f32[512,512]{1,0:T(8,128)}, f32[512,512]{1,0:T(8,128)S(1)}, u32[]{:S(2)}) copy-start(f32[512,512]{1,0:T(8,128)S(1)} %multiply_add_fusion) | copy-start | bytes 3145732
  180.6 3.7 copy-start.3
  180.6 3.7 copy-start.38
  186.6 2.6 copy-start.9
  186.6 3.9 copy-start.28
  266.4 22.1 %copy-start.13 = (f32[7,512]{1,0:T(8,128)S(1)}, f32[7,512]{1,0:T(8,128)}, u32[]{:S(2)}) copy-start(f32[7,512]{1,0:T(8,128)} %slice.495) | copy-start | bytes 43012
  281.4 13.4 %copy-start.10 = (f32[63,512]{1,0:T(8,128)S(1)}, f32[63,512]{1,0:T(8,128)}, u32[]{:S(2)}) copy-start(f32[63,512]{1,0:T(8,128)} %slice.477) | copy-start | bytes 387076
  289.2 6.5 %copy-start.25 = (f32[1,512]{1,0:T(1,128)S(1)}, f32[1,512]{1,0:T(1,128)}, u32[]{:S(2)}) copy-start(f32[1,512]{1,0:T(1,128)} %slice.603) | copy-start | bytes 6148
  289.9 6.6 %copy-start.5 = (f32[127,512]{1,0:T(8,128)S(1)}, f32[127,512]{1,0:T(8,128)}, u32[]{:S(2)}) copy-start(f32[127,512]{1,0:T(8,128)} %slice.528) | copy-start | bytes 780292
  289.9 6.6 %copy-start.6 = (f32[127,512]{1,0:T(8,128)S(1)}, f32[127,512]{1,0:T(8,128)}, u32[]{:S(2)}) copy-start(f32[127,512]{1,0:T(8,128)} %slice.471) | copy-start | bytes 780292
  293.1 3.5 copy-start.24
  298.7 6.1 copy-start.23
  303.3 4.4 copy-start.16
  303.3 5.2 copy-start.17
  304.8 2.9 copy-start.19
  304.8 2.9 copy-start.20
  304.8 2.9 copy-start.21
  304.8 2.9 copy-start.22
  304.8 3.7 copy-start.18
  304.8 3.7 copy-start.30
  304.8 3.8 copy-start.14
  304.8 3.8 copy-start.15
  304.8 3.8 copy-start.29
  304.9 7.1 %copy-start.11 = (f32[63,512]{1,0:T(8,128)S(1)}, f32[63,512]{1,0:T(8,128)}, u32[]{:S(2)}) copy-start(f32[63,512]{1,0:T(8,128)} %slice.547) | copy-start | bytes 387076
  304.9 7.1 %copy-start.12 = (f32[63,512]{1,0:T(8,128)S(1)}, f32[63,512]{1,0:T(8,128)}, u32[]{:S(2)}) copy-start(f32[63,512]{1,0:T(8,128)} %slice.596) | copy-start | bytes 387076
  308.7 4.8 copy-start.7
  311.9 1.7 copy-start.27
  315.7 6.1 copy-start.26
  324.5 11.8 %copy-start.1 = (f32[512,512]{1,0:T(8,128)S(1)}, f32[512,512]{1,0:T(8,128)}, u32[]{:S(2)}) copy-start(f32[512,512]{1,0:T(8,128)} %pad.132) | copy-start | bytes 3145732
  341.1 132.6 %all-gather.11.cloned.1.call-start = ((), (), s32[]{:S(2)}) async-start(), calls=%async_computation.3 | async-start | bytes 5242880 | tf_op jit(solution)/shard_map/all_gather | solution.py:95
  344.0 3.1 copy-start.34
  344.0 15.1 %copy-start.33 = (f32[1024]{0:T(1024)S(1)}, f32[1024]{0:T(1024)}, u32[]{:S(2)}) copy-start(f32[1024]{0:T(1024)} %param.27) | copy-start | bytes 12292
  344.0 210.4 %all-gather.13.cloned.1.call-start = ((), (), s32[]{:S(2)}) async-start(), calls=%async_computation.4 | async-start | bytes 5242880 | tf_op jit(solution)/shard_map/all_gather | solution.py:100
  347.0 267.4 %all-reduce.42.cloned.1.call-start = ((), (), s32[]{:S(2)}) async-start(), calls=%async_computation.5 | async-start | bytes 4194304 | tf_op jit(solution)/shard_map/psum | solution.py:103
  391.5 163.0 %copy-start.40 = (f32[2048]{0:T(1024)S(1)}, f32[2048]{0:T(1024)}, u32[]{:S(2)}) copy-start(f32[2048]{0:T(1024)} %param.25) | copy-start | bytes 24580
  564.4 0.7 copy-start.35
Sparse Core Ops, SparseCore 0:
  8.9 48.3 all-gather.6
  58.9 44.4 all-gather.8
  341.3 50.1 all-reduce.39
  392.9 80.8 all-gather.10
  475.2 79.2 all-gather.12
  564.5 49.8 all-reduce.41
where the time goes:
time: 633 us; the launch traced here: 626 us
  waiting for transfers between devices  277 us (44%)
  local copies, waits for them, and re-layouts  205 us (32%)
  other arithmetic  76.6 us (12%)
  matrix products  29.3 us (5%)
  blocking collectives  23.9 us (4%)
  between operations  14.3 us (2%)
    slice x106, local copies, waits for them, and re-layouts, one_direction(): carried = lax.associative_scan(combine_steps, (decay, drive), axis=0)  159 us
    all_gather x1, waiting for transfers between devices, body(): lax.all_gather(down_matrix.astype(jnp.bfloat16), 'fs', axis=0, tiled=True)  80.7 us
    all_gather x1, waiting for transfers between devices, body(): lax.all_gather(up_matrix.astype(jnp.bfloat16), 'fs', axis=0, tiled=True)  79.8 us
    all_gather x1, waiting for transfers between devices, body(): lax.all_gather(in_matrix.astype(jnp.bfloat16), 'fs', axis=0, tiled=True)  46.4 us
    psum x1, waiting for transfers between devices, body(): lax.psum(lowered.astype(jnp.bfloat16), 'tp').astype(jnp.float32)  37.4 us
    psum x1, waiting for transfers between devices, body(): lax.psum(partial_value.astype(jnp.bfloat16), 'tp').astype(jnp.float32)  32.4 us
    mul x14, other arithmetic, combine_steps(): return (earlier[0] * later[0], later[0] * earlier[1] + later[1])  24.4 us
    pad x32, local copies, waits for them, and re-layouts, one_direction(): carried = lax.associative_scan(combine_steps, (decay, drive), axis=0)  18.9 us
  transfers between devices with their start and end apart: 6, of which 5 were waited for; matrix products, arithmetic and copies ran while one was open for 46% of the time, Pallas kernels for 0%

commit v1 on v0

v1 whole, which is shorter than its diff:
```python
import functools
import jax
import jax.numpy as jnp
from jax import lax
from jax.experimental import pallas as pl
from jax.experimental.pallas import tpu as pltpu
from jax.sharding import PartitionSpec as P

EPSILON = 1e-06
RATE_GAIN = 8.0
LANES = 128
SEGMENTS = 8
PAD = 8


def normalize(stream, gain):
    return stream * lax.rsqrt(jnp.mean(stream * stream, axis=-1, keepdims=True) + EPSILON) * gain


def one_minus_exp(y):
    series = 1.0 + y * (1.0 / 6.0)
    for k in (5.0, 4.0, 3.0, 2.0):
        series = 1.0 + y * (1.0 / k) * series
    return jnp.where(y > -0.25, -y * series, 1.0 - jnp.exp(y))


def sigmoid(x):
    return 0.5 * jnp.tanh(0.5 * x) + 0.5


def recurrence_kernel(before_ref, taps_ref, rate_ref, recall_ref, admit_ref, mixed_ref, padded, decay, drive, prefix):
    length, width = before_ref.shape
    directions, groups, block, _ = recall_ref.shape
    taps = taps_ref.shape[0]
    chunks = width // LANES
    steps = length // SEGMENTS

    edge = jnp.zeros((PAD, width), jnp.float32)
    padded[pl.ds(0, PAD), :] = edge
    padded[pl.ds(PAD + length, PAD), :] = edge
    padded[pl.ds(PAD, length), :] = before_ref[...].astype(jnp.float32)

    rows = length // SEGMENTS
    weights = [
        [(recall_ref[d, g].astype(jnp.bfloat16), admit_ref[d, g].astype(jnp.bfloat16)) for g in range(groups)]
        for d in range(directions)
    ]

    for tile in range(SEGMENTS):
        base = tile * rows
        conv = taps_ref[0:1, :] * padded[pl.ds(base + PAD - taps // 2, rows), :]
        for k in range(1, taps):
            conv = conv + taps_ref[k : k + 1, :] * padded[pl.ds(base + PAD - taps // 2 + k, rows), :]
        narrow = conv.astype(jnp.bfloat16)
        for g in range(groups):
            values = conv[:, g * block : (g + 1) * block]
            left = narrow[:, g * block : (g + 1) * block]
            for d in range(directions):
                recall_map, admit_map = weights[d][g]
                recall = sigmoid(jnp.dot(left, recall_map, preferred_element_type=jnp.float32))
                admit = sigmoid(jnp.dot(left, admit_map, preferred_element_type=jnp.float32))
                log_decay = recall * (-RATE_GAIN * rate_ref[d : d + 1, g * block : (g + 1) * block])
                a = jnp.exp(log_decay)
                b = jnp.sqrt(one_minus_exp(2.0 * log_decay)) * admit * values
                for c in range(block // LANES):
                    where = g * (block // LANES) + c
                    decay[d, where, pl.ds(base, rows), :] = a[:, c * LANES : (c + 1) * LANES]
                    drive[d, where, pl.ds(base, rows), :] = b[:, c * LANES : (c + 1) * LANES]

    lanes = [(d, c) for d in range(directions) for c in range(chunks)]

    def scan_step(s, carried):
        out = []
        for (d, c), (state, product) in zip(lanes, carried):
            at = s if d == 0 else steps - 1 - s
            a = decay[d, c, pl.ds(at, SEGMENTS, stride=steps), :]
            b = drive[d, c, pl.ds(at, SEGMENTS, stride=steps), :]
            state = a * state + b
            product = a * product
            drive[d, c, pl.ds(at, SEGMENTS, stride=steps), :] = state
            prefix[d, c, pl.ds(at, SEGMENTS, stride=steps), :] = product
            out.append((state, product))
        return tuple(out)

    start = tuple((jnp.zeros((SEGMENTS, LANES), jnp.float32), jnp.ones((SEGMENTS, LANES), jnp.float32)) for _ in lanes)
    ends = lax.fori_loop(0, steps, scan_step, start, unroll=4)
    ends = dict(zip(lanes, ends))

    for c in range(chunks):
        carries = []
        for d in range(directions):
            state, product = ends[(d, c)]
            order = range(SEGMENTS) if d == 0 else range(SEGMENTS - 1, -1, -1)
            carry = jnp.zeros((1, LANES), jnp.float32)
            entering = {}
            for k in order:
                entering[k] = carry
                carry = product[k : k + 1, :] * carry + state[k : k + 1, :]
            carries.append(entering)
        for k in range(SEGMENTS):
            span = pl.ds(k * steps, steps)
            total = drive[0, c, span, :] + prefix[0, c, span, :] * carries[0][k]
            total = total + (drive[1, c, span, :] + prefix[1, c, span, :] * carries[1][k])
            mixed_ref[span, c * LANES : (c + 1) * LANES] = total.astype(jnp.bfloat16)


def recurrence(before, taps, rates, recall_maps, admit_maps):
    length, width = before.shape
    directions = rates.shape[0]
    chunks = width // LANES
    plane = pltpu.VMEM((directions, chunks, length, LANES), jnp.float32)
    return pl.pallas_call(
        recurrence_kernel,
        out_shape=jax.ShapeDtypeStruct((length, width), jnp.bfloat16),
        in_specs=[pl.BlockSpec(memory_space=pltpu.VMEM)] * 5,
        out_specs=pl.BlockSpec(memory_space=pltpu.VMEM),
        scratch_shapes=[pltpu.VMEM((length + 2 * PAD, width), jnp.float32), plane, plane, plane],
        compiler_params=pltpu.CompilerParams(vmem_limit_bytes=24 * 2**20),
        cost_estimate=pl.CostEstimate(flops=16 * length * width * 256, bytes_accessed=8 * 2**20, transcendentals=8 * length * width),
        name="recurrence",
    )(before, taps, rates, recall_maps, admit_maps)


def contract_last(left, right):
    return lax.dot_general(
        left, right, (((1,), (1,)), ((), ())), preferred_element_type=jnp.float32
    )


def gather(shard):
    copies = lax.axis_size("rep")
    if shard.shape[0] % (16 * copies):
        return lax.all_gather(shard.astype(jnp.bfloat16), "fs", axis=0, tiled=True)
    rows = shard.shape[0] // copies
    part = lax.dynamic_slice_in_dim(shard, lax.axis_index("rep") * rows, rows, 0)
    return lax.all_gather(part.astype(jnp.bfloat16), ("fs", "rep"), axis=0, tiled=True)


def body(
    tokens,
    first_gain,
    in_matrix,
    in_scale,
    conv_taps,
    decay_rate,
    recall_maps,
    admit_maps,
    out_matrix,
    out_scale,
    second_gain,
    up_matrix,
    up_scale,
    down_matrix,
    down_scale,
):
    stream = tokens.reshape(tokens.shape[1], tokens.shape[2]).astype(jnp.float32)
    factors = lax.all_gather(
        jnp.stack([out_scale, down_scale]).astype(jnp.bfloat16), "fs", axis=1, tiled=True
    )
    in_cols = gather(in_matrix)
    normed = normalize(stream, first_gain).astype(jnp.bfloat16)
    before = (
        jnp.dot(normed, in_cols, preferred_element_type=jnp.float32) * in_scale.astype(jnp.bfloat16)
    ).astype(jnp.bfloat16)
    mixed = recurrence(before, conv_taps, decay_rate, recall_maps, admit_maps)
    partial_value = contract_last(mixed, gather(out_matrix))
    middle = stream + factors[0] * lax.psum(partial_value.astype(jnp.bfloat16), "tp").astype(
        jnp.float32
    )
    second_normed = normalize(middle, second_gain).astype(jnp.bfloat16)
    raised = jnp.dot(second_normed, gather(up_matrix), preferred_element_type=jnp.float32)
    active = jnp.square(jax.nn.relu(raised * up_scale.astype(jnp.bfloat16))).astype(jnp.bfloat16)
    lowered = contract_last(active, gather(down_matrix))
    result = (
        middle + factors[1] * lax.psum(lowered.astype(jnp.bfloat16), "tp").astype(jnp.float32)
    ).astype(jnp.bfloat16)
    return result.reshape(tokens.shape)


def solution(mesh):
    placed = (
        P(("rep", "fs"), None, None),
        P(),
        P("fs", "tp"),
        P("tp"),
        P(None, "tp"),
        P(None, "tp"),
        P(None, "tp", None, None),
        P(None, "tp", None, None),
        P("fs", "tp"),
        P("fs"),
        P(),
        P("fs", "tp"),
        P("tp"),
        P("fs", "tp"),
        P("fs"),
    )
    return jax.shard_map(
        body, mesh=mesh, in_specs=placed, out_specs=P(("rep", "fs"), None, None), check_vma=False
    )
```

time: 633 us -> 387 us (0.61); the launches traced: 626 us -> 387 us
  local copies, waits for them, and re-layouts: 205 us -> 6.75 us
  other arithmetic: 76.6 us -> 11 us
  waiting for transfers between devices: 277 us -> 314 us
  blocking collectives: 23.9 us -> 12.1 us
  matrix products: 29.3 us -> 18.4 us
  Pallas kernels: 0 us -> 10.3 us
    slice x107 -> x0, local copies, waits for them, and re-layouts: 159 us -> none  [the longest x106 159 us: one_direction(): carried = lax.associative_scan(combine_steps, (decay, drive), axis=0)]
    mul x15 -> x1, other arithmetic: 25 us -> 0.01 us  [body(): factors[1]]
    all_gather x4, waiting for transfers between devices: 207 us -> 230 us  [gather(): lax.all_gather(part.astype(jnp.bfloat16), ('fs', 'rep'), axis=0, tiled=True)]
    pad x32 -> x0, local copies, waits for them, and re-layouts: 18.9 us -> none  [one_direction(): carried = lax.associative_scan(combine_steps, (decay, drive), axis=0)]
    add x36 -> x0, other arithmetic: 18.2 us -> none  [the longest x18 10.4 us: combine_steps(): return (earlier[0] * later[0], later[0] * earlier[1] + later[1])]
    rev x2 -> x0, local copies, waits for them, and re-layouts: 15.8 us -> none  [the longest x1 8.95 us: recurrence(): one_direction(values[::-1], rates[1], recall_maps[1], admit_maps[1])[::-1]]
    psum x1, waiting for transfers between devices: 37.4 us -> 50 us  [body(): lax.psum(lowered.astype(jnp.bfloat16), 'tp').astype(jnp.float32)]
    all_gather x2 -> x1, blocking collectives: 23.9 us -> 12.1 us  [body(): lax.all_gather(jnp.stack([out_scale, down_scale]).astype(jnp.bfloat16), '...]
  transfers between devices with their start and end apart: 6 -> 6, of which waited for: 5 -> 6; matrix products, arithmetic and copies ran while one was open for 46% -> 4% of each run, Pallas kernels for 0% -> 3%
where the time goes in v1:
time: 387 us
  waiting for transfers between devices  314 us (81%)
  matrix products  18.4 us (5%)
  between operations  13.6 us (4%)
  blocking collectives  12.1 us (3%)
  other arithmetic  11 us (3%)
  Pallas kernels  10.3 us (3%)
  local copies, waits for them, and re-layouts  6.75 us (2%)
    all_gather x4, waiting for transfers between devices, gather(): lax.all_gather(part.astype(jnp.bfloat16), ('fs', 'rep'), axis=0, tiled=True)  230 us
    psum x1, waiting for transfers between devices, body(): lax.psum(lowered.astype(jnp.bfloat16), 'tp').astype(jnp.float32)  50 us
    psum x1, waiting for transfers between devices, body(): lax.psum(partial_value.astype(jnp.bfloat16), 'tp').astype(jnp.float32)  34.6 us
    dot_general x2, matrix products, contract_last(): lax.dot_general(left, right, (((1,), (1,)), ((), ())), preferred_element_...  14.7 us
    all_gather x1, blocking collectives, body(): lax.all_gather(jnp.stack([out_scale, down_scale]).astype(jnp.bfloat16), '...  12.1 us
    pallas_call x1, Pallas kernels, recurrence(): pl.pallas_call(recurrence_kernel, out_shape=jax.ShapeDtypeStruct((length,...  10.3 us
  transfers between devices with their start and end apart: 6, of which 6 were waited for; matrix products, arithmetic and copies ran while one was open for 4% of the time, Pallas kernels for 3%

profile of v1, /device:TPU:0, one launch (start us, length us, event | category | flops | bytes accessed | tf_op | source)
XLA Modules:
  0.0 386.8 jit_solution(12792690212202219649)
XLA Ops:
  6.5 0.0 copy-start
  6.5 0.0 copy-start.8
  6.5 0.0 copy-start.9
  6.5 0.0 all-gather.5.cloned.1.call-start
  6.6 1.9 dynamic-slice_convert_fusion.3
  8.5 0.0 all-gather.5.cloned.1.call-update
  8.5 0.0 all-gather.7.cloned.1.call-start
  8.6 1.8 dynamic-slice_convert_fusion.2
  10.3 0.0 all-gather.7.cloned.1.call-update
  10.4 0.0 all-reduce.3.cloned.1.call-start
  10.4 2.1 fusion
  12.5 0.0 copy-done.8
  12.5 48.8 %all-gather.5.cloned.1.call-done = bf16[2048,512]{1,0:T(8,128)(2,1)} async-done(((bf16[256,512]{1,0:T(8,128)(2,1)}), bf16[2048,512]{1,0:T(8,128)(2,1)}) %all-gather.5.cloned.1.call-update) | async-done | bytes 2097168 | tf_op jit(solution)/shard_map/all_gather | solution.py:136
  61.3 0.0 copy-done.9
  61.3 0.0 copy-start.1
  61.3 0.0 copy-start.2
  61.3 0.0 copy-start.3
  61.3 0.0 copy-start.4
  61.3 3.7 fusion.17.before_ref
  65.0 0.0 copy-done.1
  65.0 0.0 copy-done.2
  65.0 0.0 copy-done.3
  65.0 0.0 copy-done.4
  65.0 10.3 %recurrence.1 = bf16[512,512]{1,0:T(8,128)(2,1)S(1)} custom-call(bf16[512,512]{1,0:T(8,128)(2,1)S(1)} %fusion.17.before_ref, f32[4,512]{1,0:T(4,128)S(1)} %copy-done.3, f32[2,512]{1,0:T(2,128)S(1)} %copy-done.4, f32[2,2,256,256]{3,2,1,0:T(8,128)S(1)} %copy-done.1, f32[2,2,256,256]{3,2,1,0:T(8,128)S(1)} %copy-done.2), custom_call_target="tpu_custom_call" | custom-call | flops 1073741824 | bytes 8388608 | tf_op jit(solution)/shard_map/recurrence/pallas_call | solution.py:112
  75.4 35.7 %all-gather.7.cloned.1.call-done = bf16[2048,512]{1,0:T(8,128)(2,1)} async-done(((bf16[256,512]{1,0:T(8,128)(2,1)}), bf16[2048,512]{1,0:T(8,128)(2,1)}) %all-gather.7.cloned.1.call-update) | async-done | bytes 2097168 | tf_op jit(solution)/shard_map/all_gather | solution.py:136
  111.1 4.2 %convolution_convert_fusion.1 = bf16[512,2048]{1,0:T(8,128)(2,1)} fusion(bf16[512,512]{1,0:T(8,128)(2,1)S(1)} %recurrence.1, bf16[2048,512]{1,0:T(8,128)(2,1)} %all-gather.7.cloned.1.call-done), kind=kOutput, calls=%fused_computation.10 | convolution fusion | flops 1074790400 | bytes 4718592 | tf_op jit(solution)/shard_map/dot_general | solution.py:125
  115.3 0.0 all-reduce.3.cloned.1.call-update
  115.3 0.0 copy-start.6
  115.3 0.0 copy-start.7
  115.3 0.0 copy-start.5
  115.3 0.0 all-gather.9.cloned.1.call-start
  115.4 0.0 copy-done
  115.4 0.9 dynamic-slice_convert_fusion.1
  116.3 0.0 all-gather.9.cloned.1.call-update
  116.3 0.0 all-gather.11.cloned.1.call-start
  116.3 2.1 dynamic-slice_convert_fusion
  118.4 0.0 all-gather.11.cloned.1.call-update
  118.5 0.0 all-reduce.5.cloned.1.call-start
  118.5 0.0 copy-done.6
  118.5 0.0 copy-done.7
  118.6 12.1 %all_gather.15 = bf16[2,2048]{1,0:T(2,128)(2,1)S(1)} all-gather(bf16[2,512]{1,0:T(2,128)(2,1)S(1)} %pad_maximum_fusion), channel_id=1, replica_groups=mesh['rep'=2,'fs'=4,'tp'=4] {'fs'}, dimensions={1}, use_global_device_ids=true | all-gather | bytes 10240 | tf_op jit(solution)/shard_map/all_gather | solution.py:157
  130.7 0.0 copy-done.5
  130.7 34.6 %all-reduce.3.cloned.1.call-done = bf16[512,2048]{1,0:T(8,128)(2,1)} async-done(((bf16[512,2048]{1,0:T(8,128)(2,1)}), bf16[512,2048]{1,0:T(8,128)(2,1)}) %all-reduce.3.cloned.1.call-update) | async-done | bytes 2097168 | tf_op jit(solution)/shard_map/psum | solution.py:167
  165.4 0.0 copy-start.10
  165.4 3.1 multiply_reduce_fusion
  168.5 71.8 %all-gather.9.cloned.1.call-done = bf16[2048,1024]{1,0:T(8,128)(2,1)} async-done(((bf16[256,1024]{1,0:T(8,128)(2,1)}), bf16[2048,1024]{1,0:T(8,128)(2,1)}) %all-gather.9.cloned.1.call-update) | async-done | bytes 4194320 | tf_op jit(solution)/shard_map/all_gather | solution.py:136
  240.3 73.3 %all-gather.11.cloned.1.call-done = bf16[2048,1024]{1,0:T(8,128)(2,1)} async-done(((bf16[256,1024]{1,0:T(8,128)(2,1)}), bf16[2048,1024]{1,0:T(8,128)(2,1)}) %all-gather.11.cloned.1.call-update) | async-done | bytes 4194320 | tf_op jit(solution)/shard_map/all_gather | solution.py:136
  313.6 0.0 copy-done.10
  313.6 10.5 %convolution_convert_fusion = bf16[512,2048]{1,0:T(8,128)(2,1)} fusion(bf16[2048,1024]{1,0:T(8,128)(2,1)} %all-gather.11.cloned.1.call-done, bf16[2048,1024]{1,0:T(8,128)(2,1)} %all-gather.9.cloned.1.call-done, bf16[512,2048]{1,0:T(8,128)(2,1)} %all-reduce.3.cloned.1.call-done, bf16[1,512,2048]{2,1,0:T(8,128)(2,1)} %param.15, f32[2048]{0:T(1024)S(1)} %copy-done.10, ...), kind=kOutput, calls=%fused_computation.9 | convolution fusion | flops 4305453056 | bytes 14702592 | tf_op jit(solution)/shard_map/dot_general | solution.py:125
  324.1 0.0 all-reduce.5.cloned.1.call-update
  324.2 50.0 %all-reduce.5.cloned.1.call-done = bf16[512,2048]{1,0:T(8,128)(2,1)} async-done(((bf16[512,2048]{1,0:T(8,128)(2,1)}), bf16[512,2048]{1,0:T(8,128)(2,1)}) %all-reduce.5.cloned.1.call-update) | async-done | bytes 2097168 | tf_op jit(solution)/shard_map/psum | solution.py:175
  374.2 5.7 %fusion.4 = bf16[1,512,2048]{2,1,0:T(8,128)(2,1)} fusion(bf16[512,2048]{1,0:T(8,128)(2,1)} %all-reduce.5.cloned.1.call-done, bf16[512,2048]{1,0:T(8,128)(2,1)} %all-reduce.3.cloned.1.call-done, bf16[1,512,2048]{2,1,0:T(8,128)(2,1)} %param.15, f32[2048]{0:T(1024)S(1)} %bitcast.33, f32[2048]{0:T(1024)S(1)} %bitcast.32), kind=kLoop, calls=%fused_computation.12 | loop fusion | flops 8388608 | bytes 8404992 | tf_op jit(solution)/shard_map/reshape | solution.py:177
  (9 shorter events, 0.1 us)
Async XLA Ops:
  6.5 108.9 %copy-start = (f32[512,1024]{1,0:T(8,128)S(1)}, f32[512,1024]{1,0:T(8,128)}, u32[]{:S(2)}) copy-start(f32[512,1024]{1,0:T(8,128)} %param.26) | copy-start | bytes 6291460
  6.5 6.0 %copy-start.8 = (f32[512]{0:T(512)S(1)}, f32[512]{0:T(512)}, u32[]{:S(2)}) copy-start(f32[512]{0:T(512)} %param.18) | copy-start | bytes 6148
  6.5 54.8 %copy-start.9 = (f32[2048]{0:T(1024)S(1)}, f32[2048]{0:T(1024)}, u32[]{:S(2)}) copy-start(f32[2048]{0:T(1024)} %param.16) | copy-start | bytes 24580
  6.5 54.8 %all-gather.5.cloned.1.call-start = ((), (), s32[]{:S(2)}) async-start(), calls=%async_computation | async-start | bytes 2359296 | tf_op jit(solution)/shard_map/all_gather | solution.py:136
  8.5 102.6 %all-gather.7.cloned.1.call-start = ((), (), s32[]{:S(2)}) async-start(), calls=%async_computation.1 | async-start | bytes 2359296 | tf_op jit(solution)/shard_map/all_gather | solution.py:136
  10.4 155.0 %all-reduce.3.cloned.1.call-start = ((), (), s32[]{:S(2)}) async-start(), calls=%async_computation.2 | async-start | bytes 4194304 | tf_op jit(solution)/shard_map/psum | solution.py:167
  61.3 3.7 copy-start.1
  61.3 3.7 copy-start.2
  61.3 3.7 copy-start.3
  61.3 3.7 copy-start.4
  115.3 3.2 copy-start.6
  115.3 3.2 copy-start.7
  115.3 15.4 %copy-start.5 = (f32[1024]{0:T(1024)S(1)}, f32[1024]{0:T(1024)}, u32[]{:S(2)}) copy-start(f32[1024]{0:T(1024)} %param.27) | copy-start | bytes 12292
  115.3 124.9 %all-gather.9.cloned.1.call-start = ((), (), s32[]{:S(2)}) async-start(), calls=%async_computation.3 | async-start | bytes 4718592 | tf_op jit(solution)/shard_map/all_gather | solution.py:136
  116.3 197.3 %all-gather.11.cloned.1.call-start = ((), (), s32[]{:S(2)}) async-start(), calls=%async_computation.4 | async-start | bytes 4718592 | tf_op jit(solution)/shard_map/all_gather | solution.py:136
  118.5 255.7 %all-reduce.5.cloned.1.call-start = ((), (), s32[]{:S(2)}) async-start(), calls=%async_computation.5 | async-start | bytes 4194304 | tf_op jit(solution)/shard_map/psum | solution.py:175
  165.4 148.2 %copy-start.10 = (f32[2048]{0:T(1024)S(1)}, f32[2048]{0:T(1024)}, u32[]{:S(2)}) copy-start(f32[2048]{0:T(1024)} %param.25) | copy-start | bytes 24580
Sparse Core Ops, SparseCore 0:
  9.5 51.7 all-gather.4
  63.4 47.6 all-gather.6
  115.4 49.9 all-reduce.2
  167.4 72.8 all-gather.8
  242.2 71.3 all-gather.10
  324.3 49.8 all-reduce.4

commit v2 on v1

--- a/solution.py
+++ b/solution.py
@@ -28,37 +28,25 @@
     return 0.5 * jnp.tanh(0.5 * x) + 0.5
 
 
-def recurrence_kernel(before_ref, taps_ref, rate_ref, recall_ref, admit_ref, mixed_ref, padded, decay, drive, prefix):
-    length, width = before_ref.shape
+def gate_part(padded, taps_ref, rate_ref, recall_ref, admit_ref, decay, drive, length):
     directions, groups, block, _ = recall_ref.shape
     taps = taps_ref.shape[0]
-    chunks = width // LANES
-    steps = length // SEGMENTS
-
-    edge = jnp.zeros((PAD, width), jnp.float32)
-    padded[pl.ds(0, PAD), :] = edge
-    padded[pl.ds(PAD + length, PAD), :] = edge
-    padded[pl.ds(PAD, length), :] = before_ref[...].astype(jnp.float32)
-
     rows = length // SEGMENTS
-    weights = [
-        [(recall_ref[d, g].astype(jnp.bfloat16), admit_ref[d, g].astype(jnp.bfloat16)) for g in range(groups)]
-        for d in range(directions)
-    ]
-
-    for tile in range(SEGMENTS):
-        base = tile * rows
-        conv = taps_ref[0:1, :] * padded[pl.ds(base + PAD - taps // 2, rows), :]
-        for k in range(1, taps):
-            conv = conv + taps_ref[k : k + 1, :] * padded[pl.ds(base + PAD - taps // 2 + k, rows), :]
+
+    def tile_step(tile, _):
+        base = pl.multiple_of(tile * rows, rows)
+        conv = jnp.zeros((rows, padded.shape[1]), jnp.float32)
+        window = padded[pl.ds(base, rows + 2 * PAD), :]
+        for k in range(taps):
+            first = PAD - taps // 2 + k
+            conv = conv + taps_ref[k : k + 1, :] * window[first : first + rows, :]
         narrow = conv.astype(jnp.bfloat16)
         for g in range(groups):
             values = conv[:, g * block : (g + 1) * block]
             left = narrow[:, g * block : (g + 1) * block]
             for d in range(directions):
-                recall_map, admit_map = weights[d][g]
-                recall = sigmoid(jnp.dot(left, recall_map, preferred_element_type=jnp.float32))
-                admit = sigmoid(jnp.dot(left, admit_map, preferred_element_type=jnp.float32))
+                recall = sigmoid(jnp.dot(left, recall_ref[d, g].astype(jnp.bfloat16), preferred_element_type=jnp.float32))
+                admit = sigmoid(jnp.dot(left, admit_ref[d, g].astype(jnp.bfloat16), preferred_element_type=jnp.float32))
                 log_decay = recall * (-RATE_GAIN * rate_ref[d : d + 1, g * block : (g + 1) * block])
                 a = jnp.exp(log_decay)
                 b = jnp.sqrt(one_minus_exp(2.0 * log_decay)) * admit * values
@@ -66,7 +54,14 @@
                     where = g * (block // LANES) + c
                     decay[d, where, pl.ds(base, rows), :] = a[:, c * LANES : (c + 1) * LANES]
                     drive[d, where, pl.ds(base, rows), :] = b[:, c * LANES : (c + 1) * LANES]
-
+        return 0
+
+    lax.fori_loop(0, SEGMENTS, tile_step, 0)
+
+
+def scan_part(decay, drive, prefix, mixed_ref, length):
+    directions, chunks = decay.shape[:2]
+    steps = length // SEGMENTS
     lanes = [(d, c) for d in range(directions) for c in range(chunks)]
 
     def scan_step(s, carried):
@@ -102,6 +97,16 @@
             total = drive[0, c, span, :] + prefix[0, c, span, :] * carries[0][k]
             total = total + (drive[1, c, span, :] + prefix[1, c, span, :] * carries[1][k])
             mixed_ref[span, c * LANES : (c + 1) * LANES] = total.astype(jnp.bfloat16)
+
+
+def recurrence_kernel(before_ref, taps_ref, rate_ref, recall_ref, admit_ref, mixed_ref, padded, decay, drive, prefix):
+    length, width = before_ref.shape
+    edge = jnp.zeros((PAD, width), jnp.float32)
+    padded[pl.ds(0, PAD), :] = edge
+    padded[pl.ds(PAD + length, PAD), :] = edge
+    padded[pl.ds(PAD, length), :] = before_ref[...].astype(jnp.float32)
+    gate_part(padded, taps_ref, rate_ref, recall_ref, admit_ref, decay, drive, length)
+    scan_part(decay, drive, prefix, mixed_ref, length)
 
 
 def recurrence(before, taps, rates, recall_maps, admit_maps):
@@ -176,6 +181,276 @@
     ).astype(jnp.bfloat16)
     return result.reshape(tokens.shape)
 
+MESH = pl.DeviceIdType.MESH
+
+
+def layer_kernel(
+    names, tokens_ref, first_ref, in_ref, in_scale_ref, taps_ref, rate_ref, recall_ref, admit_ref,
+    out_ref, second_ref, up_ref, up_scale_ref, down_ref, scales_ref,
+    result_ref,
+    in_all, out_all, up_all, down_all, scales_all, normed, padded, decay, drive, prefix, mixed, active,
+    first_parts, first_sums, second_parts, second_sums, middle, send, recv,
+):
+    replica, place, rank = (lax.axis_index(name) for name in names)
+    rep_name, fs_name, tp_name = names
+    fs, tp = 4, 4
+    length, model = tokens_ref.shape
+    rows = length // tp
+    block = model // fs
+    right, left, across = (lax.rem(place + k, fs) for k in (1, 3, 2))
+    mate = 1 - replica
+    near = rank + 1 - 2 * lax.rem(rank, 2)
+    far = lax.rem(rank + 2, tp)
+    count = [0]
+
+    def copy(src, dst, axis, peer):
+        index = count[0]
+        count[0] += 1
+        return pltpu.make_async_remote_copy(
+            src_ref=src, dst_ref=dst, send_sem=send.at[index], recv_sem=recv.at[index],
+            device_id={axis: peer}, device_id_type=MESH,
+        )
+
+    started = []
+
+    def start(*copies):
+        for one in copies:
+            one.start()
+            started.append(one)
+
+    class Gather:
+        def __init__(self, whole):
+            def view(owner, offset, size):
+                return whole.at[pl.ds(pl.multiple_of(owner * block + replica * half + offset, quarter), size), :]
+
+            half, quarter = block // 2, block // 4
+            own = view(place, 0, half)
+            from_left, from_right = view(left, 0, half), view(right, 0, half)
+            self.to_right = copy(own, own, fs_name, right)
+            self.to_left = copy(own, own, fs_name, left)
+            low, high = view(left, 0, quarter), view(right, quarter, quarter)
+            self.on_right = copy(low, low, fs_name, right)
+            self.on_left = copy(high, high, fs_name, left)
+            opposite = view(across, 0, half)
+            self.swaps = [copy(part, part, rep_name, mate) for part in (from_left, from_right, opposite)]
+
+        def first(self):
+            start(self.to_right, self.to_left)
+
+        def second(self):
+            self.to_right.wait_recv()
+            start(self.on_right, self.swaps[0])
+            self.to_left.wait_recv()
+            start(self.on_left, self.swaps[1])
+
+        def third(self):
+            self.on_right.wait_recv()
+            self.on_left.wait_recv()
+            start(self.swaps[2])
+
+        def finish(self):
+            for swap in self.swaps:
+                swap.wait_recv()
+
+    barrier = pltpu.get_barrier_semaphore()
+    greeted = [(rep_name, mate), (fs_name, right), (fs_name, left), (fs_name, across)]
+    greeted += [(tp_name, lax.rem(rank + k, tp)) for k in range(1, tp)]
+    for axis, peer in greeted:
+        pl.semaphore_signal(barrier, inc=1, device_id={axis: peer}, device_id_type=MESH)
+
+    own_rows = pl.ds(pl.multiple_of(place * block, block), block)
+    for shard, whole in ((in_ref, in_all), (out_ref, out_all), (up_ref, up_all), (down_ref, down_all)):
+        whole[own_rows, :] = shard[...].astype(jnp.bfloat16)
+    scales_all[place] = scales_ref[...]
+    pl.semaphore_wait(barrier, len(greeted))
+
+    g_in, g_out, g_up, g_down = (Gather(whole) for whole in (in_all, out_all, up_all, down_all))
+    g_in.first()
+    scale_copies = [
+        copy(scales_ref, scales_all.at[place], fs_name, lax.rem(place + k, fs)) for k in range(1, fs)
+    ]
+    start(*scale_copies)
+    g_out.first()
+
+    tile = 64
+
+    def norm_step(i, _):
+        at = pl.ds(pl.multiple_of(i * tile, tile), tile)
+        normed[at, :] = normalize(tokens_ref[at, :].astype(jnp.float32), first_ref[...]).astype(jnp.bfloat16)
+        return 0
+
+    lax.fori_loop(0, length // tile, norm_step, 0)
+
+    g_in.second()
+    g_in.third()
+    g_out.second()
+    g_up.first()
+    g_in.finish()
+
+    edge = jnp.zeros((PAD, padded.shape[1]), jnp.float32)
+    padded[pl.ds(0, PAD), :] = edge
+    padded[pl.ds(PAD + length, PAD), :] = edge
+    wide = 256
+
+    def in_step(i, _):
+        at = pl.ds(pl.multiple_of(i * wide, wide), wide)
+        product = jnp.dot(normed[...], in_all[:, at], preferred_element_type=jnp.float32)
+        product = product * in_scale_ref[:, at].astype(jnp.bfloat16).astype(jnp.float32)
+        padded[pl.ds(PAD, length), at] = product.astype(jnp.bfloat16).astype(jnp.float32)
+        return 0
+
+    lax.fori_loop(0, in_all.shape[1] // wide, in_step, 0)
+    g_out.third()
+    gate_part(padded, taps_ref, rate_ref, recall_ref, admit_ref, decay, drive, length)
+    g_up.second()
+    g_down.first()
+    scan_part(decay, drive, prefix, mixed, length)
+    g_up.third()
+    g_out.finish()
+    for one in scale_copies:
+        one.wait_recv()
+
+    def project(values, whole, parts, sums, between):
+        hops = []
+
+        def send_block(j):
+            hop = []
+            for k in range(1, tp):
+                peer = lax.rem(rank + k, tp)
+                hop.append(copy(parts.at[j, pl.ds(pl.multiple_of(peer * rows, rows), rows), :], sums.at[k - 1, j], tp_name, peer))
+            start(*hop)
+            hops.append(hop)
+
+        for j in range(fs):
+            def step(i, _):
+                at = pl.ds(pl.multiple_of(i * wide, wide), wide)
+                matrix = whole[pl.ds(pl.multiple_of(j * block + i * wide, wide), wide), :]
+                parts[j, :, at] = contract_last(values[...], matrix).astype(jnp.bfloat16)
+                return 0
+
+            lax.fori_loop(0, block // wide, step, 0)
+            if j:
+                send_block(j - 1)
+            between(j)
+        send_block(fs - 1)
+        return hops
+
+    own_quarter = pl.ds(pl.multiple_of(rank * rows, rows), rows)
+
+    def summed(parts, sums, hops, j):
+        for hop in hops[j]:
+            hop.wait_recv()
+        total = parts[j, own_quarter, :].astype(jnp.float32)
+        for k in range(tp - 1):
+            total = total + sums[k, j].astype(jnp.float32)
+        return total
+
+    def factor(j, which):
+        return scales_all[j, which : which + 1, :].astype(jnp.bfloat16).astype(jnp.float32)
+
+    def advance(j):
+        if j == 1:
+            g_down.second()
+
+    hops = project(mixed, out_all, first_parts, first_sums, advance)
+    squares = jnp.zeros((rows, 1), jnp.float32)
+    for j in range(fs):
+        columns = slice(j * block, (j + 1) * block)
+        value = tokens_ref[own_quarter, columns].astype(jnp.float32) + factor(j, 0) * summed(first_parts, first_sums, hops, j)
+        middle[:, columns] = value
+        squares = squares + jnp.sum(value * value, axis=1, keepdims=True)
+    inverse = lax.rsqrt(squares * (1.0 / model) + EPSILON)
+    normed[own_quarter, :] = (middle[...] * inverse * second_ref[...]).astype(jnp.bfloat16)
+
+    def spread(ref, columns):
+        own = ref.at[own_quarter, columns]
+        theirs = ref.at[pl.ds(pl.multiple_of(far * rows, rows), rows), columns]
+        return copy(own, own, tp_name, far), copy(own, own, tp_name, near), copy(theirs, theirs, tp_name, near)
+
+    whole_width = pl.ds(0, model)
+    to_far, to_near, onward = spread(normed, whole_width)
+    g_up.finish()
+    start(to_far, to_near)
+    g_down.third()
+    to_far.wait_recv()
+    start(onward)
+    to_near.wait_recv()
+    onward.wait_recv()
+
+    def up_step(i, _):
+        at = pl.ds(pl.multiple_of(i * wide, wide), wide)
+        raised = jnp.dot(normed[...], up_all[:, at], preferred_element_type=jnp.float32)
+        raised = raised * up_scale_ref[:, at].astype(jnp.bfloat16).astype(jnp.float32)
+        active[:, at] = jnp.square(jnp.maximum(raised, 0.0)).astype(jnp.bfloat16)
+        return 0
+
+    lax.fori_loop(0, up_all.shape[1] // wide, up_step, 0)
+    g_down.finish()
+    hops = project(active, down_all, second_parts, second_sums, lambda j: None)
+    spreads = []
+    for j in range(fs):
+        columns = slice(j * block, (j + 1) * block)
+        value = middle[:, columns] + factor(j, 1) * summed(second_parts, second_sums, hops, j)
+        result_ref[own_quarter, columns] = value.astype(jnp.bfloat16)
+        spreads.append(spread(result_ref, pl.ds(j * block, block)))
+        start(*spreads[j][:2])
+        if j:
+            spreads[j - 1][0].wait_recv()
+            start(spreads[j - 1][2])
+    spreads[-1][0].wait_recv()
+    start(spreads[-1][2])
+    for _, to_near, onward in spreads:
+        to_near.wait_recv()
+        onward.wait_recv()
+    for one in started:
+        one.wait_send()
+
+
+def fused_body(
+    tokens, first_gain, in_matrix, in_scale, conv_taps, decay_rate, recall_maps, admit_maps,
+    out_matrix, out_scale, second_gain, up_matrix, up_scale, down_matrix, down_scale,
+):
+    length, model = tokens.shape[1:]
+    width, hidden = in_matrix.shape[1], up_matrix.shape[1]
+    fs, tp = lax.axis_size("fs"), lax.axis_size("tp")
+    rows, block = length // tp, model // fs
+    directions = decay_rate.shape[0]
+    plane = pltpu.VMEM((directions, width // LANES, length, LANES), jnp.float32)
+    parts = pltpu.VMEM((fs, length, block), jnp.bfloat16)
+    sums = pltpu.VMEM((tp - 1, fs, rows, block), jnp.bfloat16)
+    copies = 4 * 7 + 3 + 2 * 12 + 3 + 12
+    result = pl.pallas_call(
+        functools.partial(layer_kernel, ("rep", "fs", "tp")),
+        out_shape=jax.ShapeDtypeStruct((length, model), jnp.bfloat16),
+        in_specs=[pl.BlockSpec(memory_space=pltpu.VMEM)] * 14,
+        out_specs=pl.BlockSpec(memory_space=pltpu.VMEM),
+        scratch_shapes=[
+            pltpu.VMEM((model, width), jnp.bfloat16),
+            pltpu.VMEM((model, width), jnp.bfloat16),
+            pltpu.VMEM((model, hidden), jnp.bfloat16),
+            pltpu.VMEM((model, hidden), jnp.bfloat16),
+            pltpu.VMEM((fs, 2, block), jnp.float32),
+            pltpu.VMEM((length, model), jnp.bfloat16),
+            pltpu.VMEM((length + 2 * PAD, width), jnp.float32),
+            plane, plane, plane,
+            pltpu.VMEM((length, width), jnp.bfloat16),
+            pltpu.VMEM((length, hidden), jnp.bfloat16),
+            parts, sums, parts, sums,
+            pltpu.VMEM((rows, model), jnp.float32),
+            pltpu.SemaphoreType.DMA((copies,)),
+            pltpu.SemaphoreType.DMA((copies,)),
+        ],
+        compiler_params=pltpu.CompilerParams(
+            collective_id=0, has_side_effects=True, vmem_limit_bytes=61 * 2**20
+        ),
+        name="layer",
+    )(
+        tokens.reshape(length, model), first_gain[None], in_matrix, in_scale[None], conv_taps, decay_rate,
+        recall_maps, admit_maps, out_matrix, second_gain[None], up_matrix, up_scale[None], down_matrix,
+        jnp.stack([out_scale, down_scale]),
+    )
+    return result.reshape(tokens.shape)
+
 
 def solution(mesh):
     placed = (
@@ -195,6 +470,7 @@
         P("fs", "tp"),
         P("fs"),
     )
+    small = (mesh.shape["rep"], mesh.shape["fs"], mesh.shape["tp"]) == (2, 4, 4)
     return jax.shard_map(
-        body, mesh=mesh, in_specs=placed, out_specs=P(("rep", "fs"), None, None), check_vma=False
-    )
+        fused_body if small else body, mesh=mesh, in_specs=placed, out_specs=P(("rep", "fs"), None, None), check_vma=False
+    )

time: 387 us -> 183 us (0.47)
  waiting for transfers between devices: 314 us -> 0 us
  Pallas kernels: 10.3 us -> 179 us
  matrix products: 18.4 us -> 0 us
  between operations: 13.6 us -> 0.01 us
  blocking collectives: 12.1 us -> 0 us
  other arithmetic: 11 us -> 1.3 us
    all_gather x4 -> x0, waiting for transfers between devices: 230 us -> none  [gather(): lax.all_gather(part.astype(jnp.bfloat16), ('fs', 'rep'), axis=0, tiled=True)]
    pallas_call x1, Pallas kernels: 10.3 us -> 179 us  [fused_body(): pl.pallas_call(functools.partial(layer_kernel, ('rep', 'fs', 'tp')), out_...]
    psum x2 -> x0, waiting for transfers between devices: 84.7 us -> none  [the longest x1 50 us: body(): lax.psum(lowered.astype(jnp.bfloat16), 'tp').astype(jnp.float32)]
    dot_general x3 -> x0, matrix products: 18.4 us -> none  [the longest x2 14.7 us: contract_last(): lax.dot_general(left, right, (((1,), (1,)), ((), ())), preferred_element_...]
    all_gather x1 -> x0, blocking collectives: 12.1 us -> none  [body(): lax.all_gather(jnp.stack([out_scale, down_scale]).astype(jnp.bfloat16), '...]
    convert_element_type x4 -> x0, local copies, waits for them, and re-layouts: 6.68 us -> none  [gather(): part.astype(jnp.bfloat16)]
    reshape x1 -> x0, other arithmetic: 5.72 us -> none  [body(): return result.reshape(tokens.shape)]
    reduce_sum x2 -> x0, other arithmetic: 5.2 us -> none  [normalize(): jnp.mean(stream * stream, axis=-1, keepdims=True) + EPSILON]
  transfers between devices with their start and end apart: 6 -> 0, of which waited for: 6 -> 0; matrix products, arithmetic and copies ran while one was open for 4% -> 0% of each run, Pallas kernels for 3% -> 0%
where the time goes in v2:
time: 183 us
  Pallas kernels  179 us (98%)
  local copies, waits for them, and re-layouts  3.16 us (2%)
    pallas_call x1, Pallas kernels, fused_body(): pl.pallas_call(functools.partial(layer_kernel, ('rep', 'fs', 'tp')), out_...  179 us

profile of v2, /device:TPU:0, one launch (start us, length us, event | category | flops | bytes accessed | tf_op | source)
XLA Modules:
  0.0 183.2 jit_solution(7191453015904008897)
XLA Ops:
  0.0 1.3 pad_maximum_fusion.scales_ref
  1.3 178.7 %layer.1 = bf16[512,2048]{1,0:T(8,128)(2,1)} custom-call(bf16[512,2048]{1,0:T(8,128)(2,1)} %bitcast.9, f32[1,2048]{1,0:T(1,128)} %bitcast.10, f32[512,512]{1,0:T(8,128)} %in_ref.1, f32[1,512]{1,0:T(1,128)} %bitcast.13, f32[4,512]{1,0:T(4,128)} %taps_ref.1, f32[2,512]{1,0:T(2,128)} %rate_ref.1, f32[2,2,256,256]{3,2,1,0:T(8,128)} %recall_ref.1, ...), custom_call_target="tpu_custom_call" | custom-call | tf_op jit(solution)/shard_map/layer/pallas_call | solution.py:422
  180.0 3.2 %copy.17 = bf16[1,512,2048]{2,1,0:T(8,128)(2,1)} copy(bf16[1,512,2048]{2,1,0:T(8,128)(2,1)} %bitcast.8) | data formatting | bytes 4194304

commit v3 on v2

--- a/solution.py
+++ b/solution.py
@@ -306,11 +306,12 @@
     g_down.first()
     scan_part(decay, drive, prefix, mixed, length)
     g_up.third()
-    g_out.finish()
     for one in scale_copies:
         one.wait_recv()
 
-    def project(values, whole, parts, sums, between):
+    order = (place, left, right, across)
+
+    def project(gathered, values, whole, parts, sums, between):
         hops = []
 
         def send_block(j):
@@ -322,9 +323,12 @@
             hops.append(hop)
 
         for j in range(fs):
+            if j:
+                gathered.swaps[j - 1].wait_recv()
+
             def step(i, _):
                 at = pl.ds(pl.multiple_of(i * wide, wide), wide)
-                matrix = whole[pl.ds(pl.multiple_of(j * block + i * wide, wide), wide), :]
+                matrix = whole[pl.ds(pl.multiple_of(order[j] * block + i * wide, wide), wide), :]
                 parts[j, :, at] = contract_last(values[...], matrix).astype(jnp.bfloat16)
                 return 0
 
@@ -346,16 +350,16 @@
         return total
 
     def factor(j, which):
-        return scales_all[j, which : which + 1, :].astype(jnp.bfloat16).astype(jnp.float32)
+        return scales_all[order[j], which : which + 1, :].astype(jnp.bfloat16).astype(jnp.float32)
 
     def advance(j):
         if j == 1:
             g_down.second()
 
-    hops = project(mixed, out_all, first_parts, first_sums, advance)
+    hops = project(g_out, mixed, out_all, first_parts, first_sums, advance)
     squares = jnp.zeros((rows, 1), jnp.float32)
     for j in range(fs):
-        columns = slice(j * block, (j + 1) * block)
+        columns = pl.ds(pl.multiple_of(order[j] * block, block), block)
         value = tokens_ref[own_quarter, columns].astype(jnp.float32) + factor(j, 0) * summed(first_parts, first_sums, hops, j)
         middle[:, columns] = value
         squares = squares + jnp.sum(value * value, axis=1, keepdims=True)
@@ -369,11 +373,13 @@
 
     whole_width = pl.ds(0, model)
     to_far, to_near, onward = spread(normed, whole_width)
-    g_up.finish()
+    g_up.swaps[0].wait_recv()
     start(to_far, to_near)
-    g_down.third()
     to_far.wait_recv()
     start(onward)
+    g_down.third()
+    g_up.swaps[1].wait_recv()
+    g_up.swaps[2].wait_recv()
     to_near.wait_recv()
     onward.wait_recv()
 
@@ -385,14 +391,13 @@
         return 0
 
     lax.fori_loop(0, up_all.shape[1] // wide, up_step, 0)
-    g_down.finish()
-    hops = project(active, down_all, second_parts, second_sums, lambda j: None)
+    hops = project(g_down, active, down_all, second_parts, second_sums, lambda j: None)
     spreads = []
     for j in range(fs):
-        columns = slice(j * block, (j + 1) * block)
+        columns = pl.ds(pl.multiple_of(order[j] * block, block), block)
         value = middle[:, columns] + factor(j, 1) * summed(second_parts, second_sums, hops, j)
         result_ref[own_quarter, columns] = value.astype(jnp.bfloat16)
-        spreads.append(spread(result_ref, pl.ds(j * block, block)))
+        spreads.append(spread(result_ref, columns))
         start(*spreads[j][:2])
         if j:
             spreads[j - 1][0].wait_recv()

time: 183 us -> 183 us (level)
  no operation moved by 1% of the time
where the time goes in v3:
time: 183 us
  Pallas kernels  179 us (98%)
  local copies, waits for them, and re-layouts  3.16 us (2%)
    pallas_call x1, Pallas kernels, fused_body(): pl.pallas_call(functools.partial(layer_kernel, ('rep', 'fs', 'tp')), out_...  179 us

profile of v3, /device:TPU:0, one launch (start us, length us, event | category | flops | bytes accessed | tf_op | source)
XLA Modules:
  0.0 183.2 jit_solution(826296130815615763)
XLA Ops:
  0.0 1.3 pad_maximum_fusion.scales_ref
  1.3 178.7 %layer.1 = bf16[512,2048]{1,0:T(8,128)(2,1)} custom-call(bf16[512,2048]{1,0:T(8,128)(2,1)} %bitcast.9, f32[1,2048]{1,0:T(1,128)} %bitcast.10, f32[512,512]{1,0:T(8,128)} %in_ref.1, f32[1,512]{1,0:T(1,128)} %bitcast.13, f32[4,512]{1,0:T(4,128)} %taps_ref.1, f32[2,512]{1,0:T(2,128)} %rate_ref.1, f32[2,2,256,256]{3,2,1,0:T(8,128)} %recall_ref.1, ...), custom_call_target="tpu_custom_call" | custom-call | tf_op jit(solution)/shard_map/layer/pallas_call | solution.py:427
  180.0 3.2 %copy.17 = bf16[1,512,2048]{2,1,0:T(8,128)(2,1)} copy(bf16[1,512,2048]{2,1,0:T(8,128)(2,1)} %bitcast.8) | data formatting | bytes 4194304
